TPU v7x, 32 devices: a whole 2x2x4 slice. The times are simulated.
32 devices in a mesh: grp: 2 (over y), sp: 4 (over z), tp: 4 (over x, core).
Axes of the slice: x: 2, y: 2, z: 4, core: 2. Of those that a mesh axis runs over, the one named last changes fastest.
Arguments:
- query_nope: bfloat16 [2560, 1024], P(('grp', 'sp'), 'tp'), parts along dimension 0, may hold values from -12 to 12
- query_rope: bfloat16 [2560, 512], P(('grp', 'sp'), 'tp'), parts along dimension 0, may hold values from -48 to 48
- token_latent: bfloat16 [2560, 256], P(('grp', 'sp')), parts along dimension 0, may hold values from -6 to 6
- key_rope: bfloat16 [2560, 32], P(('grp', 'sp')), parts along dimension 0, may hold values from -48 to 48
- latent_norm_gain: float32 [256], replicated, may hold values from 0.1 to 1.9
- key_expand_weight: bfloat16 [256, 1024], replicated, may hold values from -0.375 to 0.375
- value_expand_weight: bfloat16 [256, 1024], replicated, may hold values from -0.375 to 0.375
- residual: bfloat16 [2560, 2048], P(('grp', 'sp')), parts along dimension 0, may hold values from -3 to 3
- out_weight: bfloat16 [1024, 2048], P('tp'), may hold values from -0.375 to 0.375
- ffn_gain: float32 [2048], replicated, may hold values from 0.1 to 1.9
- gate_weight: bfloat16 [2048, 5632], P('sp', 'tp'), may hold values from -0.125 to 0.125
- up_weight: bfloat16 [2048, 5632], P('sp', 'tp'), may hold values from -0.125 to 0.125
- down_weight: bfloat16 [5632, 2048], P('tp', 'sp'), may hold values from -0.078125 to 0.078125
Outputs:
- layer_output: bfloat16 [2560, 2048], P(('grp', 'sp', 'tp')), parts along dimension 0
There are 2 independent parts, one for each index of `grp`. A program takes and returns all parts, laid end to end along the dimension named above; an argument that names none is the same for every part. Nothing has to cross between parts.
All inputs are finite; a program needn't handle non-finite values.
Results may differ from a plain program's by a relative error of at most 0.015.
Values may be sent and summed in bfloat16 or wider, within the bound.
A program may use at most 128 MiB of HBM per device.

v0:
```python
import jax
import jax.numpy as jnp
from jax import lax
from jax.sharding import PartitionSpec as P

UNROTATED_SIZE = 64
ROPE = 32
VALUE_SIZE = 64
GRID_W = 64


def norm_rows(values, gain):
    wide = values.astype(jnp.float32)
    return wide * lax.rsqrt(jnp.mean(wide * wide, axis=-1, keepdims=True) + 1e-06) * gain


def turn_heads(vectors, positions):
    tokens, heads, width = vectors.shape
    freqs = width // 4
    grid_pos = jnp.stack([positions // GRID_W, positions % GRID_W], axis=-1).astype(jnp.float32)
    inverse = jnp.power(10000.0, -jnp.arange(freqs, dtype=jnp.float32) / freqs)
    angles = grid_pos[:, :, None] * inverse
    cosine = jnp.cos(angles)[:, None]
    sine = jnp.sin(angles)[:, None]
    viewed = vectors.reshape(tokens, heads, 2, 2, freqs)
    first = viewed[..., 0, :]
    second = viewed[..., 1, :]
    turned = jnp.stack([first * cosine - second * sine, first * sine + second * cosine], axis=-2)
    return turned.reshape(tokens, heads, width)


def local(
    query_nope,
    query_rope,
    token_latent,
    key_rope,
    latent_norm_gain,
    key_expand_weight,
    value_expand_weight,
    residual,
    out_weight,
    ffn_gain,
    gate_weight,
    up_weight,
    down_weight,
):
    tok_rows = query_nope.shape[0]
    heads_here = query_nope.shape[1] // UNROTATED_SIZE
    own_rows = tok_rows // lax.axis_size("tp")
    tp_index = lax.axis_index("tp")
    positions = lax.axis_index("sp") * tok_rows + jnp.arange(tok_rows, dtype=jnp.int32)
    query_flat = query_nope.reshape(tok_rows, heads_here, UNROTATED_SIZE)
    query_turned = turn_heads(
        query_rope.astype(jnp.float32).reshape(tok_rows, heads_here, ROPE), positions
    ).astype(jnp.bfloat16)
    latent = norm_rows(token_latent, latent_norm_gain).astype(jnp.bfloat16)
    key_turned = turn_heads(key_rope.astype(jnp.float32)[:, None, :], positions)[:, 0].astype(
        jnp.bfloat16
    )
    key_cols = lax.dynamic_slice_in_dim(
        key_expand_weight, tp_index * heads_here * UNROTATED_SIZE, heads_here * UNROTATED_SIZE, 1
    )
    value_cols = lax.dynamic_slice_in_dim(
        value_expand_weight, tp_index * heads_here * VALUE_SIZE, heads_here * VALUE_SIZE, 1
    )
    score_scale = (UNROTATED_SIZE + ROPE) ** (-0.5)

    def absorb(carried, block_in):
        latent_block, rope_block = block_in
        block_rows = latent_block.shape[0]
        key_rows = jnp.dot(latent_block, key_cols, preferred_element_type=jnp.float32).astype(
            jnp.bfloat16
        )
        key_rows = key_rows.reshape(block_rows, heads_here, UNROTATED_SIZE)
        value_rows = jnp.dot(latent_block, value_cols, preferred_element_type=jnp.float32).astype(
            jnp.bfloat16
        )
        value_rows = value_rows.reshape(block_rows, heads_here, VALUE_SIZE)
        scores = (
            jnp.einsum("qhd,khd->hqk", query_flat, key_rows, preferred_element_type=jnp.float32)
            + jnp.einsum(
                "qhd,kd->hqk", query_turned, rope_block, preferred_element_type=jnp.float32
            )
        ) * score_scale
        highest, totals, accumulated = carried
        new_highest = jnp.maximum(highest, jnp.max(scores, axis=-1))
        shrink = jnp.exp(highest - new_highest)
        weights = jnp.exp(scores - new_highest[:, :, None])
        totals = totals * shrink + jnp.sum(weights, axis=-1)
        accumulated = accumulated * shrink.T[:, :, None] + jnp.einsum(
            "hqk,khd->qhd",
            weights.astype(jnp.bfloat16),
            value_rows,
            preferred_element_type=jnp.float32,
        )
        return ((new_highest, totals, accumulated), None)

    initial = (
        jnp.full((heads_here, tok_rows), -jnp.inf, jnp.float32),
        jnp.zeros((heads_here, tok_rows), jnp.float32),
        jnp.zeros((tok_rows, heads_here, VALUE_SIZE), jnp.float32),
    )
    carried = initial
    latent_piece = lax.all_gather(latent, "sp", axis=0, tiled=True)
    rope_piece = lax.all_gather(key_turned, "sp", axis=0, tiled=True)
    shard_count = latent_piece.shape[0] // tok_rows
    grouped = max(
        (
            factor
            for factor in range(1, shard_count + 1)
            if shard_count % factor == 0 and factor * tok_rows <= max(1024, tok_rows)
        )
    )
    block_rows = grouped * tok_rows
    blocks = (
        latent_piece.reshape(-1, block_rows, latent_piece.shape[1]),
        rope_piece.reshape(-1, block_rows, rope_piece.shape[1]),
    )
    carried, _ = lax.scan(absorb, carried, blocks)
    highest, totals, accumulated = carried
    attended = (
        (accumulated / totals.T[:, :, None])
        .reshape(tok_rows, heads_here * VALUE_SIZE)
        .astype(jnp.bfloat16)
    )
    projected = jnp.dot(attended, out_weight, preferred_element_type=jnp.float32).astype(
        jnp.bfloat16
    )
    summed = lax.psum(projected, "tp").astype(jnp.float32)
    mixed_all = residual.astype(jnp.float32) + summed
    normed_all = norm_rows(mixed_all, ffn_gain).astype(jnp.bfloat16)
    mixed_own = lax.dynamic_slice_in_dim(mixed_all, tp_index * own_rows, own_rows, 0)
    gate_piece = lax.all_gather(gate_weight, "sp", axis=0, tiled=True)
    up_piece = lax.all_gather(up_weight, "sp", axis=0, tiled=True)
    gate = jnp.dot(normed_all, gate_piece, preferred_element_type=jnp.float32)
    up_part = jnp.dot(normed_all, up_piece, preferred_element_type=jnp.float32)
    hidden = (jax.nn.silu(gate) * up_part).astype(jnp.bfloat16)
    terms = jnp.dot(
        hidden,
        lax.all_gather(down_weight, "sp", axis=1, tiled=True),
        preferred_element_type=jnp.float32,
    )
    ffn_own = lax.psum_scatter(
        terms.astype(jnp.bfloat16), "tp", scatter_dimension=0, tiled=True
    ).astype(jnp.float32)
    return (mixed_own + ffn_own).astype(jnp.bfloat16)


def solution(mesh):
    return jax.shard_map(
        local,
        mesh=mesh,
        in_specs=(
            P(("grp", "sp"), "tp"),
            P(("grp", "sp"), "tp"),
            P(("grp", "sp"), None),
            P(("grp", "sp"), None),
            P(),
            P(),
            P(),
            P(("grp", "sp"), None),
            P("tp", None),
            P(),
            P("sp", "tp"),
            P("sp", "tp"),
            P("tp", "sp"),
        ),
        out_specs=P(("grp", "sp", "tp"), None),
        check_vma=False,
    )
```

profile of v0, /device:TPU:0, one launch (start us, length us, event | category | flops | bytes accessed | tf_op | source)
XLA Modules:
  0.0 428.1 jit_solution(11533256106749414533)
XLA Ops:
  7.4 0.0 copy-start
  7.4 0.0 all-reduce.2.cloned.1.call-start
  7.4 1.1 copy.26
  8.6 0.7 convert.18
  9.3 0.2 multiply_cosine_fusion
  9.5 0.2 fusion.32
  9.7 15.1 %all-gather = bf16[4,320,32]{1,2,0:T(8,128)(2,1)S(1)} all-gather(bf16[1,320,32]{1,2,0:T(8,128)(2,1)S(1)} %bitcast.82), channel_id=1, replica_groups=mesh['grp'=2,'sp'=4,'tp'=4] {'sp'}, dimensions={0}, use_global_device_ids=true | all-gather | bytes 102400 | tf_op jit(solution)/shard_map/all_gather | solution.py:105
  24.8 0.1 copy.25
  24.8 0.1 reshape.160
  25.0 1.1 fusion.24
  26.1 1.0 fusion.26
  27.1 16.8 %all_gather.15 = bf16[1280,256]{1,0:T(8,128)(2,1)S(1)} all-gather(bf16[320,256]{1,0:T(8,128)(2,1)S(1)} %fusion.26), channel_id=1, replica_groups=mesh['grp'=2,'sp'=4,'tp'=4] {'sp'}, dimensions={0}, use_global_device_ids=true | all-gather | bytes 819200 | tf_op jit(solution)/shard_map/all_gather | solution.py:104
  43.9 0.2 copy.24
  44.2 1.0 constant_dynamic-slice_fusion
  45.2 15.2 %while.15 = (s32[]{:T(128)}, f32[4,320]{1,0:T(4,128)S(1)}, f32[4,320]{1,0:T(4,128)S(1)}, f32[320,4,64]{0,2,1:T(8,128)S(1)}, bf16[2,640,256]{2,1,0:T(8,128)(2,1)S...) while((s32[]{:T(128)}, f32[4,320]{1,0:T(4,128)S(1)}, ...), condition=%wide.region_4.5_spmd.clone, body=%wide.region_1.4_spmd.clone.sunk | while | flops 436231680 | bytes 32759976 | solution.py:119
  45.2 0.3 convolution_convert_fusion.6
  45.5 0.6 fusion.74
  46.1 2.4 fusion.75
  48.5 0.3 convolution_convert_fusion.7
  48.8 2.9 fusion.79
  51.8 1.0 fusion.77
  52.8 0.3 convolution_convert_fusion.6
  53.1 0.6 fusion.74
  53.7 2.4 fusion.75
  56.1 0.3 convolution_convert_fusion.7
  56.4 2.9 fusion.79
  59.3 1.0 fusion.77
  60.4 1.6 convolution_convert_fusion.3
  62.0 0.0 all-reduce.2.cloned.1.call-update
  62.1 0.0 all-gather.5.cloned.1.call-start
  62.1 0.5 all-gather.5.cloned.1.call-update
  62.6 0.0 all-gather.7.cloned.1.call-start
  62.7 0.5 all-gather.7.cloned.1.call-update
  63.2 0.0 all-gather.9.cloned.1.call-start
  63.3 0.5 all-gather.9.cloned.1.call-update
  63.8 0.0 copy-start.4
  63.8 0.0 reduce-scatter.2.cloned.1.call-start
  63.9 37.3 %all-reduce.2.cloned.1.call-done = bf16[320,2048]{1,0:T(8,128)(2,1)} async-done(((bf16[320,2048]{1,0:T(8,128)(2,1)}), bf16[320,2048]{1,0:T(8,128)(2,1)}) %all-reduce.2.cloned.1.call-update) | async-done | bytes 1310736 | tf_op jit(solution)/shard_map/psum | solution.py:129
  101.1 0.0 copy-done.2
  101.1 3.2 convert_add_fusion
  104.4 66.1 %all-gather.5.cloned.1.call-done = bf16[2048,1408]{1,0:T(8,128)(2,1)} async-done(((bf16[512,1408]{1,0:T(8,128)(2,1)}), bf16[2048,1408]{1,0:T(8,128)(2,1)}) %all-gather.5.cloned.1.call-update) | async-done | bytes 5767184 | tf_op jit(solution)/shard_map/all_gather | solution.py:133
  170.5 6.5 %fusion.36 = f32[320,1408]{1,0:T(8,128)} fusion(bf16[2048,1408]{1,0:T(8,128)(2,1)} %all-gather.5.cloned.1.call-done, f32[2048]{0:T(1024)S(1)} %copy-done.4, f32[320]{0:T(512)S(1)} %add_rsqrt_fusion, bf16[320,2048]{1,0:T(8,128)(2,1)} %all-reduce.2.cloned.1.call-done, bf16[320,2048]{1,0:T(8,128)(2,1)S(1)} %copy-done.2), kind=kOutput, calls=%fused_computation.69 | convolution fusion | flops 1849425920 | bytes 10200320 | tf_op jit(solution)/shard_map/dot_general | solution.py:135
  177.0 99.7 %all-gather.7.cloned.1.call-done = bf16[2048,1408]{1,0:T(8,128)(2,1)} async-done(((bf16[512,1408]{1,0:T(8,128)(2,1)}), bf16[2048,1408]{1,0:T(8,128)(2,1)}) %all-gather.7.cloned.1.call-update) | async-done | bytes 5767184 | tf_op jit(solution)/shard_map/all_gather | solution.py:134
  276.8 106.3 %all-gather.9.cloned.1.call-done = bf16[1408,2048]{1,0:T(8,128)(2,1)} async-done(((bf16[1408,512]{1,0:T(8,128)(2,1)}), bf16[1408,2048]{1,0:T(8,128)(2,1)}) %all-gather.9.cloned.1.call-update) | async-done | bytes 5767184 | tf_op jit(solution)/shard_map/all_gather | solution.py:140
  383.0 10.7 %convolution_convert_fusion.2 = bf16[320,2048]{1,0:T(8,128)(2,1)} fusion(bf16[1408,2048]{1,0:T(8,128)(2,1)} %all-gather.9.cloned.1.call-done, bf16[2048,1408]{1,0:T(8,128)(2,1)} %all-gather.7.cloned.1.call-done, f32[320,1408]{1,0:T(8,128)} %fusion.36, f32[2048]{0:T(1024)S(1)} %copy-done.4, f32[320]{0:T(512)S(1)} %add_rsqrt_fusion, ...), kind=kOutput, calls=%fused_computation.27 | convolution fusion | flops 3698278400 | bytes 17278208 | tf_op jit(solution)/shard_map/dot_general | solution.py:138
  393.7 0.0 reduce-scatter.2.cloned.1.call-update
  393.7 24.8 %reduce-scatter.2.cloned.1.call-done = bf16[80,2048]{1,0:T(8,128)(2,1)} async-done(((bf16[320,2048]{1,0:T(8,128)(2,1)}), bf16[80,2048]{1,0:T(8,128)(2,1)}) %reduce-scatter.2.cloned.1.call-update) | async-done | bytes 327696 | tf_op jit(solution)/shard_map/reduce_scatter | solution.py:143
  418.6 2.0 add_convert_fusion
  (29 shorter events, 0.3 us)
Async XLA Ops:
  7.4 53.0 %copy-start = (bf16[256,2048]{1,0:T(8,128)(2,1)S(1)}, bf16[256,2048]{1,0:T(8,128)(2,1)}, u32[]{:S(2)}) copy-start(bf16[256,2048]{1,0:T(8,128)(2,1)} %param.23) | copy-start | bytes 3145732
  7.4 36.6 %copy-start.3 = (bf16[320,256]{1,0:T(8,128)(2,1)S(1)}, bf16[320,256]{1,0:T(8,128)(2,1)}, u32[]{:S(2)}) copy-start(bf16[320,256]{1,0:T(8,128)(2,1)} %param.15) | copy-start | bytes 491524
  7.4 93.8 %all-reduce.2.cloned.1.call-start = ((), (), s32[]{:S(2)}) async-start(), calls=%async_computation.1 | async-start | bytes 2621440 | tf_op jit(solution)/shard_map/psum | solution.py:129
  48.5 3.2 copy-start.1
  56.1 3.2 copy-start.1
  62.0 39.1 %copy-start.2 = (bf16[320,2048]{1,0:T(8,128)(2,1)S(1)}, bf16[320,2048]{1,0:T(8,128)(2,1)}, u32[]{:S(2)}) copy-start(bf16[320,2048]{1,0:T(8,128)(2,1)} %param.22) | copy-start | bytes 3932164
  62.1 108.4 %all-gather.5.cloned.1.call-start = ((), (), s32[]{:S(2)}) async-start(), calls=%async_computation.2 | async-start | bytes 7208960 | tf_op jit(solution)/shard_map/all_gather | solution.py:133
  62.6 214.1 %all-gather.7.cloned.1.call-start = ((), (), s32[]{:S(2)}) async-start(), calls=%async_computation.3 | async-start | bytes 7208960 | tf_op jit(solution)/shard_map/all_gather | solution.py:134
  63.2 319.8 %all-gather.9.cloned.1.call-start = ((), (), s32[]{:S(2)}) async-start(), calls=%async_computation.4 | async-start | bytes 7208960 | tf_op jit(solution)/shard_map/all_gather | solution.py:140
  63.8 106.7 %copy-start.4 = (f32[2048]{0:T(1024)S(1)}, f32[2048]{0:T(1024)}, u32[]{:S(2)}) copy-start(f32[2048]{0:T(1024)} %param.24) | copy-start | bytes 24580
  63.8 354.8 %reduce-scatter.2.cloned.1.call-start = ((), (), s32[]{:S(2)}) async-start(), calls=%async_computation.5 | async-start | bytes 1638400 | tf_op jit(solution)/shard_map/reduce_scatter | solution.py:143
Sparse Core Ops, SparseCore 0:
  62.2 38.9 all-reduce.1
  393.8 24.6 reduce-scatter.1
Sparse Core Ops, SparseCore 1:
  64.1 106.3 all-gather.4
  171.9 104.8 all-gather.6
  278.2 104.8 all-gather.8
where the time goes:
time: 428 us
  waiting for transfers between devices  336 us (79%)
  blocking collectives  31.9 us (7%)
  matrix products  31.9 us (7%)
  between operations  15.2 us (4%)
  other arithmetic  10.5 us (2%)
    all_gather x1, waiting for transfers between devices, local(): lax.all_gather(down_weight, 'sp', axis=1, tiled=True)  106 us
    all_gather x1, waiting for transfers between devices, local(): up_piece = lax.all_gather(up_weight, 'sp', axis=0, tiled=True)  99.7 us
    all_gather x1, waiting for transfers between devices, local(): gate_piece = lax.all_gather(gate_weight, 'sp', axis=0, tiled=True)  66.1 us
    psum x1, waiting for transfers between devices, local(): summed = lax.psum(projected, 'tp').astype(jnp.float32)  37.3 us
    reduce_scatter x1, waiting for transfers between devices, local(): lax.psum_scatter(terms.astype(jnp.bfloat16), 'tp', scatter_dimension=0, t...  24.8 us
    all_gather x1, blocking collectives, local(): latent_piece = lax.all_gather(latent, 'sp', axis=0, tiled=True)  16.8 us
    all_gather x1, blocking collectives, local(): rope_piece = lax.all_gather(key_turned, 'sp', axis=0, tiled=True)  15.1 us
    dot_general x1, matrix products, local(): jnp.dot(hidden, lax.all_gather(down_weight, 'sp', axis=1, tiled=True), pr...  10.7 us
  transfers between devices with their start and end apart: 5, of which 5 were waited for; matrix products, arithmetic and copies ran while one was open for 2% of the time, Pallas kernels for 0%

commit v1 on v0

--- a/solution.py
+++ b/solution.py
@@ -131,7 +131,12 @@
     normed_all = norm_rows(mixed_all, ffn_gain).astype(jnp.bfloat16)
     mixed_own = lax.dynamic_slice_in_dim(mixed_all, tp_index * own_rows, own_rows, 0)
     gate_piece = lax.all_gather(gate_weight, "sp", axis=0, tiled=True)
-    up_piece = lax.all_gather(up_weight, "sp", axis=0, tiled=True)
+    ring = [up_weight]
+    for hop in range(3):
+        ring.append(lax.ppermute(ring[-1], "sp", [(dev, (dev + 1) % 4) for dev in range(4)]))
+    up_piece = jnp.roll(
+        jnp.concatenate(ring[::-1], axis=0), (lax.axis_index("sp") + 1) * ring[0].shape[0], axis=0
+    )
     gate = jnp.dot(normed_all, gate_piece, preferred_element_type=jnp.float32)
     up_part = jnp.dot(normed_all, up_piece, preferred_element_type=jnp.float32)
     hidden = (jax.nn.silu(gate) * up_part).astype(jnp.bfloat16)

time: 428 us -> 387 us (0.904)
  waiting for transfers between devices: 336 us -> 259 us
  starting transfers between devices: 0.17 us -> 18.3 us
  local copies, waits for them, and re-layouts: 2.49 us -> 19.2 us
    ppermute x0 -> x3, waiting for transfers between devices: none -> 177 us  [local(): lax.ppermute(ring[-1], 'sp', [(dev, (dev + 1) % 4) for dev in range(4)])]
    all_gather x1 -> x0, waiting for transfers between devices: 99.7 us -> none  [local(): up_piece = lax.all_gather(up_weight, 'sp', axis=0, tiled=True)]
    all_gather x1, waiting for transfers between devices: 66.1 us -> 0.01 us  [local(): gate_piece = lax.all_gather(gate_weight, 'sp', axis=0, tiled=True)]
    all_gather x1, waiting for transfers between devices: 106 us -> 56.1 us  [local(): lax.all_gather(down_weight, 'sp', axis=1, tiled=True)]
    psum x1, waiting for transfers between devices: 37.3 us -> 0.01 us  [local(): summed = lax.psum(projected, 'tp').astype(jnp.float32)]
    ppermute x0 -> x3, starting transfers between devices: none -> 18.2 us  [local(): lax.ppermute(ring[-1], 'sp', [(dev, (dev + 1) % 4) for dev in range(4)])]
    unnamed x11 -> x24, local copies, waits for them, and re-layouts: 1.29 us -> 16.8 us
  transfers between devices with their start and end apart: 5 -> 7, of which waited for: 5 -> 5; matrix products, arithmetic and copies ran while one was open for 2% -> 7% of each run, Pallas kernels for 0% -> 0%
where the time goes in v1:
time: 387 us
  waiting for transfers between devices  259 us (67%)
  matrix products  32.3 us (8%)
  blocking collectives  31.9 us (8%)
  local copies, waits for them, and re-layouts  19.2 us (5%)
  starting transfers between devices  18.3 us (5%)
  between operations  15 us (4%)
  other arithmetic  11 us (3%)
    ppermute x3, waiting for transfers between devices, local(): lax.ppermute(ring[-1], 'sp', [(dev, (dev + 1) % 4) for dev in range(4)])  177 us
    all_gather x1, waiting for transfers between devices, local(): lax.all_gather(down_weight, 'sp', axis=1, tiled=True)  56.1 us
    reduce_scatter x1, waiting for transfers between devices, local(): lax.psum_scatter(terms.astype(jnp.bfloat16), 'tp', scatter_dimension=0, t...  25.4 us
    ppermute x3, starting transfers between devices, local(): lax.ppermute(ring[-1], 'sp', [(dev, (dev + 1) % 4) for dev in range(4)])  18.2 us
    all_gather x1, blocking collectives, local(): latent_piece = lax.all_gather(latent, 'sp', axis=0, tiled=True)  16.8 us
    unnamed x24, local copies, waits for them, and re-layouts  16.8 us
    all_gather x1, blocking collectives, local(): rope_piece = lax.all_gather(key_turned, 'sp', axis=0, tiled=True)  15.1 us
    dot_general x1, matrix products, local(): jnp.dot(hidden, lax.all_gather(down_weight, 'sp', axis=1, tiled=True), pr...  10.6 us
  transfers between devices with their start and end apart: 7, of which 5 were waited for; matrix products, arithmetic and copies ran while one was open for 7% of the time, Pallas kernels for 0%

profile of v1, /device:TPU:0, one launch (start us, length us, event | category | flops | bytes accessed | tf_op | source)
XLA Modules:
  0.0 387.0 jit_solution(5197179331423233158)
XLA Ops:
  7.4 1.1 copy.26
  8.6 0.7 convert.18
  9.3 0.2 multiply_cosine_fusion
  9.5 0.2 fusion.42
  9.7 15.1 %all-gather = bf16[4,320,32]{1,2,0:T(8,128)(2,1)S(1)} all-gather(bf16[1,320,32]{1,2,0:T(8,128)(2,1)S(1)} %bitcast.81), channel_id=1, replica_groups=mesh['grp'=2,'sp'=4,'tp'=4] {'sp'}, dimensions={0}, use_global_device_ids=true | all-gather | bytes 102400 | tf_op jit(solution)/shard_map/all_gather | solution.py:105
  24.8 0.1 reshape.160
  25.0 1.1 fusion.34
  26.1 1.0 fusion.36
  27.1 16.8 %all_gather.12 = bf16[1280,256]{1,0:T(8,128)(2,1)S(1)} all-gather(bf16[320,256]{1,0:T(8,128)(2,1)S(1)} %fusion.36), channel_id=1, replica_groups=mesh['grp'=2,'sp'=4,'tp'=4] {'sp'}, dimensions={0}, use_global_device_ids=true | all-gather | bytes 819200 | tf_op jit(solution)/shard_map/all_gather | solution.py:104
  43.9 0.2 copy.24
  44.2 1.0 constant_dynamic-slice_fusion
  45.2 15.2 %while.15 = (s32[]{:T(128)}, f32[4,320]{1,0:T(4,128)S(1)}, f32[4,320]{1,0:T(4,128)S(1)}, f32[320,4,64]{0,2,1:T(8,128)S(1)}, bf16[2,640,256]{2,1,0:T(8,128)(2,1)S...) while((s32[]{:T(128)}, f32[4,320]{1,0:T(4,128)S(1)}, ...), condition=%wide.region_4.5_spmd.clone, body=%wide.region_1.4_spmd.clone.sunk | while | flops 436231680 | bytes 32759976 | solution.py:119
  45.2 0.3 convolution_convert_fusion.6
  45.5 0.6 fusion.85
  46.1 2.4 fusion.86
  48.5 0.3 convolution_convert_fusion.7
  48.8 2.9 fusion.90
  51.8 1.0 fusion.88
  52.8 0.3 convolution_convert_fusion.6
  53.1 0.6 fusion.85
  53.7 2.4 fusion.86
  56.1 0.3 convolution_convert_fusion.7
  56.4 2.9 fusion.90
  59.3 1.0 fusion.88
  60.4 1.6 convolution_convert_fusion.3
  62.1 0.5 all-gather.4.cloned.1.call-update
  62.7 0.5 all-gather.6.cloned.1.call-update
  63.4 0.1 collective-permute-start
  63.5 52.6 %collective-permute-done = bf16[512,1408]{1,0:T(8,128)(2,1)S(1)} collective-permute-done((bf16[512,1408]{1,0:T(8,128)(2,1)S(1)}, bf16[512,1408]{1,0:T(8,128)(2,1)S(1)}, u32[]{:S(2)}, u32[]{:S(2)}) %collective-permute-start) | collective-permute-done | bytes 1441824 | tf_op jit(solution)/shard_map/ppermute | solution.py:136
  116.1 1.2 copy-done.3
  117.3 13.5 %collective-permute-start.1 = (bf16[512,1408]{1,0:T(8,128)(2,1)S(1)}, bf16[512,1408]{1,0:T(8,128)(2,1)}, u32[]{:S(2)}, u32[]{:S(2)}) collective-permute-start(bf16[512,1408]{1,0:T(8,128)(2,1)S(1)} %collective-permute-done), channel_id=1, source_target_pairs={{0,4},{4,8},{8,12},{12,0},{1,5},{5,9},{9,13},{13,1},{2,6},{6,10},{... | collective-permute-start | bytes 4325384 | tf_op jit(solution)/shard_map/ppermute | solution.py:136
  130.8 75.2 %collective-permute-done.1 = bf16[512,1408]{1,0:T(8,128)(2,1)} collective-permute-done((bf16[512,1408]{1,0:T(8,128)(2,1)S(1)}, bf16[512,1408]{1,0:T(8,128)(2,1)}, u32[]{:S(2)}, u32[]{:S(2)}) %collective-permute-start.1) | collective-permute-done | bytes 1441824 | tf_op jit(solution)/shard_map/ppermute | solution.py:136
  206.0 4.5 %collective-permute-start.2 = (bf16[512,1408]{1,0:T(8,128)(2,1)}, bf16[512,1408]{1,0:T(8,128)(2,1)}, u32[]{:S(2)}, u32[]{:S(2)}) collective-permute-start(bf16[512,1408]{1,0:T(8,128)(2,1)} %collective-permute-done.1), channel_id=1, source_target_pairs={{0,4},{4,8},{8,12},{12,0},{1,5},{5,9},{9,13},{13,1},{2,6},{6,10},{... | collective-permute-start | bytes 4325384 | tf_op jit(solution)/shard_map/ppermute | solution.py:136
  210.5 3.7 convert_add_fusion
  214.2 48.7 %collective-permute-done.2 = bf16[512,1408]{1,0:T(8,128)(2,1)} collective-permute-done((bf16[512,1408]{1,0:T(8,128)(2,1)}, bf16[512,1408]{1,0:T(8,128)(2,1)}, u32[]{:S(2)}, u32[]{:S(2)}) %collective-permute-start.2) | collective-permute-done | bytes 1441824 | tf_op jit(solution)/shard_map/ppermute | solution.py:136
  263.0 2.6 constant_dynamic-update-slice_fusion.7
  265.5 2.6 constant_dynamic-update-slice_fusion.6
  268.1 1.2 constant_dynamic-update-slice_fusion.5
  269.3 1.3 constant_dynamic-update-slice_fusion.4
  270.6 2.6 constant_dynamic-update-slice_fusion.3
  273.2 2.7 constant_dynamic-update-slice_fusion.2
  275.9 1.3 constant_dynamic-update-slice_fusion.1
  277.2 1.2 constant_dynamic-update-slice_fusion
  278.4 7.1 %fusion.48 = f32[320,1408]{1,0:T(8,128)} fusion(bf16[2048,1408]{1,0:T(8,128)(2,1)} %all-gather.4.cloned.1.call-done, f32[2048]{0:T(1024)S(1)} %copy-done.7, f32[320]{0:T(512)S(1)} %add_rsqrt_fusion, bf16[320,2048]{1,0:T(8,128)(2,1)} %all-reduce.2.cloned.1.call-done, bf16[320,2048]{1,0:T(8,128)(2,1)} %param.22), kind=kOutput, calls=%fused_computation.81 | convolution fusion | flops 1849425920 | bytes 10200320 | tf_op jit(solution)/shard_map/dot_general | solution.py:140
  285.4 56.1 %all-gather.6.cloned.1.call-done = bf16[1408,2048]{1,0:T(8,128)(2,1)} async-done(((bf16[1408,512]{1,0:T(8,128)(2,1)}), bf16[1408,2048]{1,0:T(8,128)(2,1)}) %all-gather.6.cloned.1.call-update) | async-done | bytes 5767184 | tf_op jit(solution)/shard_map/all_gather | solution.py:145
  341.6 10.6 %convolution_convert_fusion.2 = bf16[320,2048]{1,0:T(8,128)(2,1)} fusion(bf16[1408,2048]{1,0:T(8,128)(2,1)} %all-gather.6.cloned.1.call-done, bf16[4096,1408]{1,0:T(8,128)(2,1)} %constant_dynamic-update-slice_fusion, s32[]{:T(128)S(6)} %select_n.57, f32[320,1408]{1,0:T(8,128)} %fusion.48, f32[2048]{0:T(1024)S(1)} %copy-done.7, f32[320]{0:T(512)S(1)} %add_rsqrt_fusion, ...), kind=kOutput, calls=%fused_computation.30 | convolution fusion | flops 3698278400 | bytes 17278212 | tf_op jit(solution)/shard_map/dot_general | solution.py:143
  352.2 25.4 %reduce-scatter.2.cloned.1.call-done = bf16[80,2048]{1,0:T(8,128)(2,1)} async-done(((bf16[320,2048]{1,0:T(8,128)(2,1)}), bf16[80,2048]{1,0:T(8,128)(2,1)}) %reduce-scatter.2.cloned.1.call-update) | async-done | bytes 327696 | tf_op jit(solution)/shard_map/reduce_scatter | solution.py:148
  377.6 2.0 add_convert_fusion
  (46 shorter events, 0.6 us)
Async XLA Ops:
  7.4 53.0 %copy-start = (bf16[256,2048]{1,0:T(8,128)(2,1)S(1)}, bf16[256,2048]{1,0:T(8,128)(2,1)}, u32[]{:S(2)}) copy-start(bf16[256,2048]{1,0:T(8,128)(2,1)} %param.23) | copy-start | bytes 3145732
  7.4 36.6 %copy-start.6 = (bf16[320,256]{1,0:T(8,128)(2,1)S(1)}, bf16[320,256]{1,0:T(8,128)(2,1)}, u32[]{:S(2)}) copy-start(bf16[320,256]{1,0:T(8,128)(2,1)} %param.15) | copy-start | bytes 491524
  7.4 203.1 %all-reduce.2.cloned.1.call-start = ((), (), s32[]{:S(2)}) async-start(), calls=%async_computation.1 | async-start | bytes 2621440 | tf_op jit(solution)/shard_map/psum | solution.py:129
  48.5 3.2 copy-start.1
  56.1 3.2 copy-start.1
  62.0 1.4 copy-start.2
  62.0 216.3 %all-gather.4.cloned.1.call-start = ((), (), s32[]{:S(2)}) async-start(), calls=%async_computation.2 | async-start | bytes 7208960 | tf_op jit(solution)/shard_map/all_gather | solution.py:133
  62.6 279.0 %all-gather.6.cloned.1.call-start = ((), (), s32[]{:S(2)}) async-start(), calls=%async_computation.3 | async-start | bytes 7208960 | tf_op jit(solution)/shard_map/all_gather | solution.py:145
  63.2 314.4 %reduce-scatter.2.cloned.1.call-start = ((), (), s32[]{:S(2)}) async-start(), calls=%async_computation.4 | async-start | bytes 1638400 | tf_op jit(solution)/shard_map/reduce_scatter | solution.py:148
  63.4 52.7 %collective-permute-start = (bf16[512,1408]{1,0:T(8,128)(2,1)S(1)}, bf16[512,1408]{1,0:T(8,128)(2,1)S(1)}, u32[]{:S(2)}, u32[]{:S(2)}) collective-permute-start(bf16[512,1408]{1,0:T(8,128)(2,1)S(1)} %copy-done.2), channel_id=1, source_target_pairs={{0,4},{4,8},{8,12},{12,0},{1,5},{5,9},{9,13},{13,1},{2,6},{6,10},{... | collective-permute-start | bytes 4325384 | tf_op jit(solution)/shard_map/ppermute | solution.py:136
  116.1 1.2 copy-start.3
  117.3 88.7 %collective-permute-start.1 = (bf16[512,1408]{1,0:T(8,128)(2,1)S(1)}, bf16[512,1408]{1,0:T(8,128)(2,1)}, u32[]{:S(2)}, u32[]{:S(2)}) collective-permute-start(bf16[512,1408]{1,0:T(8,128)(2,1)S(1)} %collective-permute-done), channel_id=1, source_target_pairs={{0,4},{4,8},{8,12},{12,0},{1,5},{5,9},{9,13},{13,1},{2,6},{6,10},{... | collective-permute-start | bytes 4325384 | tf_op jit(solution)/shard_map/ppermute | solution.py:136
  206.0 57.0 %collective-permute-start.2 = (bf16[512,1408]{1,0:T(8,128)(2,1)}, bf16[512,1408]{1,0:T(8,128)(2,1)}, u32[]{:S(2)}, u32[]{:S(2)}) collective-permute-start(bf16[512,1408]{1,0:T(8,128)(2,1)} %collective-permute-done.1), channel_id=1, source_target_pairs={{0,4},{4,8},{8,12},{12,0},{1,5},{5,9},{9,13},{13,1},{2,6},{6,10},{... | collective-permute-start | bytes 4325384 | tf_op jit(solution)/shard_map/ppermute | solution.py:136
  214.2 53.9 %copy-start.4 = (bf16[512,1408]{1,0:T(8,128)(2,1)S(1)}, bf16[512,1408]{1,0:T(8,128)(2,1)}, u32[]{:S(2)}) copy-start(bf16[512,1408]{1,0:T(8,128)(2,1)} %copy-done.3) | copy-start | bytes 4325380
  275.9 2.5 copy-start.7
  278.4 63.2 %copy-start.5 = (bf16[320,2048]{1,0:T(8,128)(2,1)S(1)}, bf16[320,2048]{1,0:T(8,128)(2,1)}, u32[]{:S(2)}) copy-start(bf16[320,2048]{1,0:T(8,128)(2,1)} %param.22) | copy-start | bytes 3932164
Sparse Core Ops, SparseCore 0:
  62.1 38.9 all-reduce.1
  352.3 25.2 reduce-scatter.1
Sparse Core Ops, SparseCore 1:
  64.1 160.0 all-gather.3
  225.6 115.9 all-gather.5
